TPU v7x, 256 devices: a 4x2x16 block of a 4x16x16 slice. The times are simulated.
256 devices in a mesh: grp: 2 (over y), fs: 16 (over z), tp: 8 (over x, core).
Axes of the slice: x: 4, y: 2, z: 16, core: 2. Of those that a mesh axis runs over, the one named last changes fastest.
The devices are a block of a 4x16x16 slice.
Arguments:
- stream_in: bfloat16 [12288, 2048], P(('grp', 'fs'), 'tp'), parts along dimension 0, may hold values from -6 to 6
- gain_before: bfloat16 [2048], P('tp'), may hold values from 0.099609375 to 1.8984375
- gain_mixer: bfloat16 [2048], P('tp'), may hold values from 0.099609375 to 1.8984375
- gain_after: bfloat16 [2048], P('tp'), may hold values from 0.099609375 to 1.8984375
- w_gate: bfloat16 [2048, 5632], P('fs', 'tp'), may hold values from -0.125 to 0.125
- w_upward: bfloat16 [2048, 5632], P('fs', 'tp'), may hold values from -0.125 to 0.125
- w_down: bfloat16 [5632, 2048], P('tp', 'fs'), may hold values from -0.078125 to 0.078125
- w_value: bfloat16 [2048, 1024], P('fs', 'tp'), may hold values from -0.125 to 0.125
- w_glu_gate: bfloat16 [2048, 1024], P('fs', 'tp'), may hold values from -0.125 to 0.125
- conv_taps: bfloat16 [31, 1024], P(None, 'tp'), may hold values from -1 to 1
- chan_gain: bfloat16 [1024], P('tp'), may hold values from 0.099609375 to 1.8984375
- chan_bias: bfloat16 [1024], P('tp'), may hold values from -3 to 3
- w_mix_out: bfloat16 [1024, 2048], P('tp', 'fs'), may hold values from -0.1875 to 0.1875
Outputs:
- stream_out: bfloat16 [12288, 2048], P(('grp', 'fs'), 'tp'), parts along dimension 0
There are 2 independent parts, one for each index of `grp`. A program takes and returns all parts, laid end to end along the dimension named above; an argument that names none is the same for every part. Nothing has to cross between parts.
All inputs are finite; a program needn't handle non-finite values.
Results may differ from a plain program's by a relative error of at most 0.017.
Values may be sent and summed in bfloat16 or wider, within the bound.
A program may use at most 64 MiB of HBM per device.

v0:
```python
import jax
import jax.numpy as jnp
from jax import lax
from jax.sharding import PartitionSpec as P

D = 2048
CHAN = 1024
KERNEL = 31
LEN = 128
epsilon = 1e-06


def from_everyone(x, axis):
    copies = jnp.broadcast_to(x, (lax.axis_size(axis), *x.shape))
    return lax.all_to_all(copies, axis, split_axis=0, concat_axis=0, tiled=True)


def over_copies(x, axis):
    return from_everyone(x, axis).sum(axis=0)


def laid_out(parts, dim):
    parts = jnp.moveaxis(parts, 0, dim)
    shape = parts.shape
    return parts.reshape(*shape[:dim], shape[dim] * shape[dim + 1], *shape[dim + 2 :])


def gathered_copies(x, axis, dim):
    return laid_out(from_everyone(x, axis), dim)


def in_blocks(x, dim, count):
    before, after = (x.shape[:dim], x.shape[dim + 1 :])
    return jnp.moveaxis(x.reshape(*before, count, -1, *after), dim, 0)


def sent_and_summed(x, axis, dim):
    parts = in_blocks(x, dim, lax.axis_size(axis))
    arrived = lax.all_to_all(parts, axis, split_axis=0, concat_axis=0, tiled=True)
    return arrived.astype(jnp.float32).sum(axis=0)


def in_one_piece(arrays, axis, dim, along):
    both = jnp.concatenate(arrays, axis=along)
    out, at, gathered = (lax.all_gather(both, axis, axis=dim, tiled=True), 0, [])
    for a in arrays:
        gathered.append(lax.slice_in_dim(out, at, at + a.shape[along], axis=along))
        at += a.shape[along]
    return tuple(gathered)


def normed_rows(stream, weights):
    values = stream.astype(jnp.float32)
    totals = over_copies(jnp.sum(values * values, axis=1), "tp")
    inverse = lax.rsqrt(totals / D + epsilon)
    scaled = (values * inverse[:, None] * weights.astype(jnp.float32)).astype(jnp.bfloat16)
    return gathered_copies(scaled, "tp", 1)


def settle(partial_term):
    return sent_and_summed(partial_term.astype(jnp.bfloat16), "tp", 1)


def pair_adder(rows, portions):
    return (
        jnp.dot(rows, portions[0], preferred_element_type=jnp.float32),
        jnp.dot(rows, portions[1], preferred_element_type=jnp.float32),
    )


def local(
    stream_in,
    gain_before,
    gain_mixer,
    gain_after,
    w_gate,
    w_upward,
    w_down,
    w_value,
    w_glu_gate,
    conv_taps,
    chan_gain,
    chan_bias,
    w_mix_out,
):
    whole_gate, whole_upward = in_one_piece((w_gate, w_upward), "fs", 0, 1)
    whole_down = lax.all_gather(w_down, "fs", axis=1, tiled=True)

    def feed_forward(rows):
        gate = jnp.dot(rows, whole_gate, preferred_element_type=jnp.float32)
        upward = jnp.dot(rows, whole_upward, preferred_element_type=jnp.float32)
        hidden = (jax.nn.silu(gate) * upward).astype(jnp.bfloat16)
        return settle(jnp.dot(hidden, whole_down, preferred_element_type=jnp.float32))

    first = (
        stream_in.astype(jnp.float32) + 0.5 * feed_forward(normed_rows(stream_in, gain_before))
    ).astype(jnp.bfloat16)
    rows = normed_rows(first, gain_mixer)
    value, gating = pair_adder(rows, in_one_piece((w_value, w_glu_gate), "fs", 0, 1))
    glued = value * jax.nn.sigmoid(gating)
    channels = glued.shape[1]
    grouped = glued.reshape(-1, LEN, channels)
    padded = jnp.pad(grouped, ((0, 0), (KERNEL - 1, 0), (0, 0)))
    taps = conv_taps.astype(jnp.float32)
    conv_sum = jnp.zeros_like(grouped)
    for lag_index in range(KERNEL):
        conv_sum = conv_sum + taps[lag_index] * padded[:, lag_index : lag_index + LEN]
    flat = conv_sum.reshape(-1, channels)
    sum_plain, sum_square = lax.psum((jnp.sum(flat, axis=1), jnp.sum(flat * flat, axis=1)), "tp")
    average = sum_plain / CHAN
    spread = sum_square / CHAN - average * average
    normed = (flat - average[:, None]) * lax.rsqrt(spread + epsilon)[:, None] * chan_gain.astype(
        jnp.float32
    ) + chan_bias.astype(jnp.float32)
    mixed = jax.nn.silu(normed).astype(jnp.bfloat16)
    branch = settle(
        jnp.dot(
            mixed,
            lax.all_gather(w_mix_out, "fs", axis=1, tiled=True),
            preferred_element_type=jnp.float32,
        )
    )
    second = (first.astype(jnp.float32) + branch).astype(jnp.bfloat16)
    third = second.astype(jnp.float32) + 0.5 * feed_forward(normed_rows(second, gain_after))
    return third.astype(jnp.bfloat16)


def solution(mesh):
    in_specs = (
        P(("grp", "fs"), "tp"),
        P("tp"),
        P("tp"),
        P("tp"),
        P("fs", "tp"),
        P("fs", "tp"),
        P("tp", "fs"),
        P("fs", "tp"),
        P("fs", "tp"),
        P(None, "tp"),
        P("tp"),
        P("tp"),
        P("tp", "fs"),
    )
    out_specs = P(("grp", "fs"), "tp")
    return jax.shard_map(local, mesh=mesh, in_specs=in_specs, out_specs=out_specs, check_vma=False)
```

profile of v0, /device:TPU:33, one launch (start us, length us, event | category | flops | bytes accessed | tf_op | source)
XLA Modules:
  0.0 407.0 jit_solution(14250651224693337071)
XLA Ops:
  6.5 0.0 all-gather.4.cloned.1.call-start
  6.6 1.8 pad_maximum_fusion
  8.4 0.1 all-gather.4.cloned.1.call-update
  8.4 0.1 all-gather.6.cloned.1.call-start
  8.5 0.7 all-gather.6.cloned.1.call-update
  9.3 1.1 fusion.33
  10.3 0.6 broadcast_in_dim.12
  10.9 23.7 %all-to-all-start = ((f32[8,1,384]{2,1,0:T(1,128)}), f32[8,1,384]{2,1,0:T(1,128)S(1)}, u32[]{:S(2)}, u32[]{:S(2)}) async-start(f32[8,1,384]{2,1,0:T(1,128)} %broadcast_in_dim.12), calls=%async_computation | async-start | bytes 24576 | tf_op jit(solution)/shard_map/all_to_all | solution.py:15
  34.6 0.7 convert_element_type.78
  35.3 4.0 all-to-all-done
  39.3 0.0 copy-done
  39.4 0.1 fusion.35
  39.5 0.2 copy.30
  39.7 0.1 broadcast_in_dim.13
  39.8 23.8 %all_to_all.48 = bf16[8,384,256]{1,2,0:T(8,128)(2,1)S(1)} all-to-all(bf16[8,384,256]{1,2,0:T(8,128)(2,1)S(1)} %broadcast_in_dim.13), channel_id=1, replica_groups=mesh['grp'=2,'fs'=16,'tp'=8] {'tp'}, dimensions={0} | all-to-all | bytes 3145728 | tf_op jit(solution)/shard_map/all_to_all | solution.py:15
  63.6 55.7 %all-gather.4.cloned.1.call-done = bf16[2048,1408]{0,1:T(8,128)(2,1)} async-done(((bf16[128,1408]{0,1:T(8,128)(2,1)}), bf16[2048,1408]{0,1:T(8,128)(2,1)}) %all-gather.4.cloned.1.call-update) | async-done | bytes 5767184 | tf_op jit(solution)/shard_map/all_gather | solution.py:45
  119.4 4.5 %fusion.4 = f32[384,704]{0,1:T(8,128)} fusion(bf16[384,2048]{0,1:T(8,128)(2,1)S(1)} %bitcast.120, bf16[2048,1408]{0,1:T(8,128)(2,1)} %all-gather.4.cloned.1.call-done), kind=kOutput, calls=%fused_computation.10 | convolution fusion | flops 1107296256 | bytes 5537792 | tf_op jit(solution)/shard_map/dot_general | solution.py:90
  123.9 75.0 %all-gather.6.cloned.1.call-done = bf16[704,2048]{1,0:T(8,128)(2,1)} async-done(((bf16[704,128]{1,0:T(8,128)(2,1)}), bf16[704,2048]{1,0:T(8,128)(2,1)}) %all-gather.6.cloned.1.call-update) | async-done | bytes 2883600 | tf_op jit(solution)/shard_map/all_gather | solution.py:87
  198.9 6.0 %convolution_convert_fusion.1 = bf16[384,2048]{1,0:T(8,128)(2,1)S(1)} fusion(bf16[704,2048]{1,0:T(8,128)(2,1)} %all-gather.6.cloned.1.call-done, bf16[384,2048]{0,1:T(8,128)(2,1)S(1)} %bitcast.121, bf16[2048,1408]{0,1:T(8,128)(2,1)} %all-gather.4.cloned.1.call-done, f32[384,704]{0,1:T(8,128)} %fusion.4), kind=kOutput, calls=%fused_computation.4 | convolution fusion | flops 2217000960 | bytes 9994240 | tf_op jit(solution)/shard_map/dot_general | solution.py:93
  205.0 1.3 copy.49
  206.3 15.6 %all-to-all-start.2 = ((bf16[8,384,256]{2,1,0:T(8,128)(2,1)}), bf16[8,384,256]{2,1,0:T(8,128)(2,1)S(1)}, u32[]{:S(2)}, u32[]{:S(2)}) async-start(bf16[8,384,256]{2,1,0:T(8,128)(2,1)} %bitcast.114), calls=%async_computation.2 | async-start | bytes 3145728 | tf_op jit(solution)/shard_map/all_to_all | solution.py:39
  221.9 0.0 all-gather.8.cloned.1.call-start
  221.9 0.0 copy-done.2
  221.9 0.0 copy-done.3
  221.9 0.6 pad_maximum_fusion.1
  222.5 0.1 all-gather.8.cloned.1.call-update
  222.6 19.8 %all-to-all-done.2 = bf16[8,384,256]{2,1,0:T(8,128)(2,1)S(1)} async-done(((bf16[8,384,256]{2,1,0:T(8,128)(2,1)}), bf16[8,384,256]{2,1,0:T(8,128)(2,1)S(1)}, u32[]{:S(2)}, u32[]{:S(2)}) %all-to-all-start.2) | async-done | bytes 1572896 | tf_op jit(solution)/shard_map/all_to_all | solution.py:39
  242.4 0.2 convert_reduce_fusion.2
  242.7 0.2 fusion.37
  242.8 0.6 broadcast_in_dim.14
  243.4 4.2 %all-to-all-start.3 = ((f32[8,1,384]{2,1,0:T(1,128)}), f32[8,1,384]{2,1,0:T(1,128)S(1)}, u32[]{:S(2)}, u32[]{:S(2)}) async-start(f32[8,1,384]{2,1,0:T(1,128)} %broadcast_in_dim.14), calls=%async_computation.3 | async-start | bytes 24576 | tf_op jit(solution)/shard_map/all_to_all | solution.py:15
  247.6 0.0 copy-done.6
  247.6 4.7 %all-to-all-done.3 = f32[8,1,384]{2,1,0:T(1,128)S(1)} async-done(((f32[8,1,384]{2,1,0:T(1,128)}), f32[8,1,384]{2,1,0:T(1,128)S(1)}, u32[]{:S(2)}, u32[]{:S(2)}) %all-to-all-start.3) | async-done | bytes 12320 | tf_op jit(solution)/shard_map/all_to_all | solution.py:15
  252.3 0.1 fusion.39
  252.5 0.2 copy.33
  252.6 1.3 broadcast_in_dim.15
  254.0 4.3 %all-to-all-start.4 = ((bf16[8,384,256]{1,2,0:T(8,128)(2,1)}), bf16[8,384,256]{1,2,0:T(8,128)(2,1)S(1)}, u32[]{:S(2)}, u32[]{:S(2)}) async-start(bf16[8,384,256]{1,2,0:T(8,128)(2,1)} %broadcast_in_dim.15), calls=%async_computation.4 | async-start | bytes 3145728 | tf_op jit(solution)/shard_map/all_to_all | solution.py:15
  258.3 0.0 copy-done.4
  258.4 26.0 %all_gather.15 = bf16[128,2048]{1,0:T(8,128)(2,1)S(1)} all-gather(bf16[128,128]{1,0:T(8,128)(2,1)S(1)} %copy-done.1), channel_id=1, replica_groups=mesh['grp'=2,'fs'=16,'tp'=8] {'fs'}, dimensions={1}, use_global_device_ids=true | all-gather | bytes 557056 | tf_op jit(solution)/shard_map/all_gather | solution.py:119
  284.5 0.0 all-to-all-done.4
  284.5 1.7 fusion.31
  286.3 0.6 fusion.23
  286.9 0.7 fusion.110
  287.6 18.3 %all-reduce.1 = (f32[384]{0:T(512)S(1)}, f32[384]{0:T(512)S(1)}) all-reduce(f32[384]{0:T(512)S(1)} %bitcast.128, f32[384]{0:T(512)S(1)} %bitcast.127), channel_id=1, replica_groups=mesh['grp'=2,'fs'=16,'tp'=8] {'tp'}, use_global_device_ids=true, to_apply=%region_8.9 | all-reduce | flops 768 | bytes 6144 | tf_op jit(solution)/shard_map/psum | solution.py:109
  306.0 0.2 multiply_convert_fusion
  306.2 0.6 convolution_convert_fusion.2
  306.7 0.1 copy.48
  306.8 23.7 %all_to_all.49 = bf16[8,384,256]{2,1,0:T(8,128)(2,1)S(1)} all-to-all(bf16[8,384,256]{2,1,0:T(8,128)(2,1)S(1)} %bitcast.116), channel_id=1, replica_groups=mesh['grp'=2,'fs'=16,'tp'=8] {'tp'}, dimensions={0} | all-to-all | bytes 3145728 | tf_op jit(solution)/shard_map/all_to_all | solution.py:39
  330.5 0.2 convert_reduce_fusion.1
  330.7 0.2 fusion.41
  330.9 0.6 broadcast_in_dim.32
  331.5 4.3 %all-to-all-start.6 = ((f32[8,1,384]{2,1,0:T(1,128)}), f32[8,1,384]{2,1,0:T(1,128)S(1)}, u32[]{:S(2)}, u32[]{:S(2)}) async-start(f32[8,1,384]{2,1,0:T(1,128)} %broadcast_in_dim.32), calls=%async_computation.6 | async-start | bytes 24576 | tf_op jit(solution)/shard_map/all_to_all | solution.py:15
  335.8 0.0 copy-done.9
  335.8 4.7 %all-to-all-done.6 = f32[8,1,384]{2,1,0:T(1,128)S(1)} async-done(((f32[8,1,384]{2,1,0:T(1,128)}), f32[8,1,384]{2,1,0:T(1,128)S(1)}, u32[]{:S(2)}, u32[]{:S(2)}) %all-to-all-start.6) | async-done | bytes 12320 | tf_op jit(solution)/shard_map/all_to_all | solution.py:15
  340.5 0.1 fusion.43
  340.7 0.2 copy.36
  340.8 0.1 broadcast_in_dim.33
  341.0 23.8 %all_to_all.50 = bf16[8,384,256]{1,2,0:T(8,128)(2,1)S(1)} all-to-all(bf16[8,384,256]{1,2,0:T(8,128)(2,1)S(1)} %broadcast_in_dim.33), channel_id=1, replica_groups=mesh['grp'=2,'fs'=16,'tp'=8] {'tp'}, dimensions={0} | all-to-all | bytes 3145728 | tf_op jit(solution)/shard_map/all_to_all | solution.py:15
  364.8 4.5 %fusion.6 = f32[384,704]{0,1:T(8,128)} fusion(bf16[384,2048]{0,1:T(8,128)(2,1)S(1)} %bitcast.122, bf16[2048,1408]{0,1:T(8,128)(2,1)} %all-gather.4.cloned.1.call-done), kind=kOutput, calls=%fused_computation.12 | convolution fusion | flops 1107296256 | bytes 5537792 | tf_op jit(solution)/shard_map/dot_general | solution.py:90
  369.3 6.0 %convolution_convert_fusion = bf16[384,2048]{1,0:T(8,128)(2,1)S(1)} fusion(bf16[704,2048]{1,0:T(8,128)(2,1)} %all-gather.6.cloned.1.call-done, bf16[384,2048]{0,1:T(8,128)(2,1)S(1)} %bitcast.123, bf16[2048,1408]{0,1:T(8,128)(2,1)} %all-gather.4.cloned.1.call-done, f32[384,704]{0,1:T(8,128)} %fusion.6), kind=kOutput, calls=%fused_computation.3 | convolution fusion | flops 2217000960 | bytes 9994240 | tf_op jit(solution)/shard_map/dot_general | solution.py:93
  375.3 0.1 copy.47
  375.4 24.1 %all_to_all.51 = bf16[8,384,256]{2,1,0:T(8,128)(2,1)S(1)} all-to-all(bf16[8,384,256]{2,1,0:T(8,128)(2,1)S(1)} %bitcast.117), channel_id=1, replica_groups=mesh['grp'=2,'fs'=16,'tp'=8] {'tp'}, dimensions={0} | all-to-all | bytes 3145728 | tf_op jit(solution)/shard_map/all_to_all | solution.py:39
  399.5 0.2 convert_reduce_fusion
  399.7 0.7 fusion.44
  (29 shorter events, 0.2 us)
Async XLA Ops:
  6.5 32.8 %copy-start = (bf16[384,256]{1,0:T(8,128)(2,1)S(1)}, bf16[384,256]{1,0:T(8,128)(2,1)}, u32[]{:S(2)}) copy-start(bf16[384,256]{1,0:T(8,128)(2,1)} %param.13) | copy-start | bytes 589828
  6.5 112.8 %all-gather.4.cloned.1.call-start = ((), (), s32[]{:S(2)}) async-start(), calls=%async_computation.9 | async-start | bytes 6127616 | tf_op jit(solution)/shard_map/all_gather | solution.py:45
  8.4 190.5 %all-gather.6.cloned.1.call-start = ((), (), s32[]{:S(2)}) async-start(), calls=%async_computation.10 | async-start | bytes 3063808 | tf_op jit(solution)/shard_map/all_gather | solution.py:87
  10.9 28.4 %all-to-all-start = ((f32[8,1,384]{2,1,0:T(1,128)}), f32[8,1,384]{2,1,0:T(1,128)S(1)}, u32[]{:S(2)}, u32[]{:S(2)}) async-start(f32[8,1,384]{2,1,0:T(1,128)} %broadcast_in_dim.12), calls=%async_computation | async-start | bytes 24576 | tf_op jit(solution)/shard_map/all_to_all | solution.py:15
  206.3 15.6 %copy-start.2 = (bf16[128,128]{1,0:T(8,128)(2,1)S(1)}, bf16[128,128]{1,0:T(8,128)(2,1)}, u32[]{:S(2)}) copy-start(bf16[128,128]{1,0:T(8,128)(2,1)} %param.21) | copy-start | bytes 98308
  206.3 15.6 %copy-start.3 = (bf16[128,128]{1,0:T(8,128)(2,1)S(1)}, bf16[128,128]{1,0:T(8,128)(2,1)}, u32[]{:S(2)}) copy-start(bf16[128,128]{1,0:T(8,128)(2,1)} %param.20) | copy-start | bytes 98308
  206.3 36.2 %all-to-all-start.2 = ((bf16[8,384,256]{2,1,0:T(8,128)(2,1)}), bf16[8,384,256]{2,1,0:T(8,128)(2,1)S(1)}, u32[]{:S(2)}, u32[]{:S(2)}) async-start(bf16[8,384,256]{2,1,0:T(8,128)(2,1)} %bitcast.114), calls=%async_computation.2 | async-start | bytes 3145728 | tf_op jit(solution)/shard_map/all_to_all | solution.py:39
  221.9 25.7 %copy-start.6 = (bf16[256]{0:T(256)(128)(2,1)S(1)}, bf16[256]{0:T(256)(128)(2,1)}, u32[]{:S(2)}) copy-start(bf16[256]{0:T(256)(128)(2,1)} %param.15) | copy-start | bytes 1540
  221.9 62.6 %all-gather.8.cloned.1.call-start = ((), (), s32[]{:S(2)}) async-start(), calls=%async_computation.11 | async-start | bytes 1114112 | tf_op jit(solution)/shard_map/all_gather | solution.py:45
  243.4 8.9 %all-to-all-start.3 = ((f32[8,1,384]{2,1,0:T(1,128)}), f32[8,1,384]{2,1,0:T(1,128)S(1)}, u32[]{:S(2)}, u32[]{:S(2)}) async-start(f32[8,1,384]{2,1,0:T(1,128)} %broadcast_in_dim.14), calls=%async_computation.3 | async-start | bytes 24576 | tf_op jit(solution)/shard_map/all_to_all | solution.py:15
  254.0 4.4 %copy-start.4 = (bf16[31,128]{1,0:T(8,128)(2,1)S(1)}, bf16[31,128]{1,0:T(8,128)(2,1)}, u32[]{:S(2)}) copy-start(bf16[31,128]{1,0:T(8,128)(2,1)} %param.22) | copy-start | bytes 23812
  254.0 4.4 %copy-start.7 = (bf16[128]{0:T(256)(128)(2,1)S(1)}, bf16[128]{0:T(256)(128)(2,1)}, u32[]{:S(2)}) copy-start(bf16[128]{0:T(256)(128)(2,1)} %param.23) | copy-start | bytes 772
  254.0 4.4 %copy-start.8 = (bf16[128]{0:T(256)(128)(2,1)S(1)}, bf16[128]{0:T(256)(128)(2,1)}, u32[]{:S(2)}) copy-start(bf16[128]{0:T(256)(128)(2,1)} %param.24) | copy-start | bytes 772
  254.0 4.4 %copy-start.1 = (bf16[128,128]{1,0:T(8,128)(2,1)S(1)}, bf16[128,128]{1,0:T(8,128)(2,1)}, u32[]{:S(2)}) copy-start(bf16[128,128]{1,0:T(8,128)(2,1)} %param.25) | copy-start | bytes 98308
  254.0 30.5 %all-to-all-start.4 = ((bf16[8,384,256]{1,2,0:T(8,128)(2,1)}), bf16[8,384,256]{1,2,0:T(8,128)(2,1)S(1)}, u32[]{:S(2)}, u32[]{:S(2)}) async-start(bf16[8,384,256]{1,2,0:T(8,128)(2,1)} %broadcast_in_dim.15), calls=%async_computation.4 | async-start | bytes 3145728 | tf_op jit(solution)/shard_map/all_to_all | solution.py:15
  284.5 1.8 copy-start.5
  330.5 5.3 %copy-start.9 = (bf16[256]{0:T(256)(128)(2,1)S(1)}, bf16[256]{0:T(256)(128)(2,1)}, u32[]{:S(2)}) copy-start(bf16[256]{0:T(256)(128)(2,1)} %param.16) | copy-start | bytes 1540
  331.5 9.0 %all-to-all-start.6 = ((f32[8,1,384]{2,1,0:T(1,128)}), f32[8,1,384]{2,1,0:T(1,128)S(1)}, u32[]{:S(2)}, u32[]{:S(2)}) async-start(f32[8,1,384]{2,1,0:T(1,128)} %broadcast_in_dim.32), calls=%async_computation.6 | async-start | bytes 24576 | tf_op jit(solution)/shard_map/all_to_all | solution.py:15
Sparse Core Ops, SparseCore 0:
  9.1 110.2 all-gather.3
  121.1 77.7 all-gather.5
  224.5 55.1 all-gather.7
where the time goes:
time: 408 us; the launch traced here: 407 us
  waiting for transfers between devices  165 us (40%)
  blocking collectives  140 us (34%)
  starting transfers between devices  52.1 us (13%)
  matrix products  24 us (6%)
  between operations  13.4 us (3%)
  other arithmetic  7.32 us (2%)
  local copies, waits for them, and re-layouts  5.53 us (1%)
    all_gather x1, waiting for transfers between devices, local(): whole_down = lax.all_gather(w_down, 'fs', axis=1, tiled=True)  75 us
    all_gather x2, waiting for transfers between devices, in_one_piece(): lax.all_gather(both, axis, axis=dim, tiled=True)  55.7 us
    all_to_all x2, blocking collectives, sent_and_summed(): lax.all_to_all(parts, axis, split_axis=0, concat_axis=0, tiled=True)  47.8 us
    all_to_all x2, blocking collectives, from_everyone(): return lax.all_to_all(copies, axis, split_axis=0, concat_axis=0, tiled=True)  47.6 us
    all_to_all x4, starting transfers between devices, from_everyone(): return lax.all_to_all(copies, axis, split_axis=0, concat_axis=0, tiled=True)  36.5 us
    all_gather x1, blocking collectives, local(): lax.all_gather(w_mix_out, 'fs', axis=1, tiled=True)  26 us
    all_to_all x1, waiting for transfers between devices, sent_and_summed(): lax.all_to_all(parts, axis, split_axis=0, concat_axis=0, tiled=True)  19.8 us
    psum x1, blocking collectives, local(): lax.psum((jnp.sum(flat, axis=1), jnp.sum(flat * flat, axis=1)), 'tp')  18.3 us
  transfers between devices with their start and end apart: 8, of which 6 were waited for; matrix products, arithmetic and copies ran while one was open for 3% of the time, Pallas kernels for 0%

commit v1 on v0

--- a/solution.py
+++ b/solution.py
@@ -113,13 +113,13 @@
         jnp.float32
     ) + chan_bias.astype(jnp.float32)
     mixed = jax.nn.silu(normed).astype(jnp.bfloat16)
-    branch = settle(
-        jnp.dot(
-            mixed,
-            lax.all_gather(w_mix_out, "fs", axis=1, tiled=True),
-            preferred_element_type=jnp.float32,
+
+    def close_the_table(x_in):
+        return jnp.concatenate(
+            lax.all_to_all(jnp.stack(lax.psum(1, "fs") * [x_in], 0), "fs", 0, 0), 1
         )
-    )
+
+    branch = settle(jnp.dot(mixed, close_the_table(w_mix_out), preferred_element_type=jnp.float32))
     second = (first.astype(jnp.float32) + branch).astype(jnp.bfloat16)
     third = second.astype(jnp.float32) + 0.5 * feed_forward(normed_rows(second, gain_after))
     return third.astype(jnp.bfloat16)

time: 408 us -> 450 us (1.10)
  waiting for transfers between devices: 165 us -> 205 us
  blocking collectives: 140 us -> 150 us
  starting transfers between devices: 52.1 us -> 43.8 us
    all_gather x2, waiting for transfers between devices: 55.7 us -> 96.1 us  [in_one_piece(): lax.all_gather(both, axis, axis=dim, tiled=True)]
    all_to_all x2 -> x3, blocking collectives: 47.8 us -> 83.7 us  [sent_and_summed(): lax.all_to_all(parts, axis, split_axis=0, concat_axis=0, tiled=True)]
    all_gather x1 -> x0, blocking collectives: 26 us -> none  [local(): lax.all_gather(w_mix_out, 'fs', axis=1, tiled=True)]
    all_to_all x1, waiting for transfers between devices: 19.8 us -> 0.01 us  [close_the_table(): lax.all_to_all(jnp.stack(lax.psum(1, 'fs') * [x_in], 0), 'fs', 0, 0)]
    all_to_all x4, waiting for transfers between devices: 13.4 us -> 33.2 us  [from_everyone(): return lax.all_to_all(copies, axis, split_axis=0, concat_axis=0, tiled=True)]
    all_to_all x1, starting transfers between devices: 15.6 us -> 7.07 us  [close_the_table(): lax.all_to_all(jnp.stack(lax.psum(1, 'fs') * [x_in], 0), 'fs', 0, 0)]
  transfers between devices with their start and end apart: 8 -> 8, of which waited for: 6 -> 7; matrix products, arithmetic and copies ran while one was open for 3% -> 3% of each run, Pallas kernels for 0% -> 0%
where the time goes in v1:
time: 450 us
  waiting for transfers between devices  205 us (46%)
  blocking collectives  150 us (33%)
  starting transfers between devices  43.8 us (10%)
  matrix products  24 us (5%)
  between operations  13.4 us (3%)
  other arithmetic  7.32 us (2%)
  local copies, waits for them, and re-layouts  5.37 us (1%)
    all_gather x2, waiting for transfers between devices, in_one_piece(): lax.all_gather(both, axis, axis=dim, tiled=True)  96.1 us
    all_to_all x3, blocking collectives, sent_and_summed(): lax.all_to_all(parts, axis, split_axis=0, concat_axis=0, tiled=True)  83.7 us
    all_gather x1, waiting for transfers between devices, local(): whole_down = lax.all_gather(w_down, 'fs', axis=1, tiled=True)  75 us
    all_to_all x2, blocking collectives, from_everyone(): return lax.all_to_all(copies, axis, split_axis=0, concat_axis=0, tiled=True)  47.6 us
    all_to_all x4, starting transfers between devices, from_everyone(): return lax.all_to_all(copies, axis, split_axis=0, concat_axis=0, tiled=True)  36.6 us
    all_to_all x4, waiting for transfers between devices, from_everyone(): return lax.all_to_all(copies, axis, split_axis=0, concat_axis=0, tiled=True)  33.2 us
    psum x1, blocking collectives, local(): lax.psum((jnp.sum(flat, axis=1), jnp.sum(flat * flat, axis=1)), 'tp')  19.1 us
    dot_general x2, matrix products, feed_forward(): jnp.dot(hidden, whole_down, preferred_element_type=jnp.float32)  12 us
  transfers between devices with their start and end apart: 8, of which 7 were waited for; matrix products, arithmetic and copies ran while one was open for 3% of the time, Pallas kernels for 0%

profile of v1, /device:TPU:33, one launch (start us, length us, event | category | flops | bytes accessed | tf_op | source)
XLA Modules:
  0.0 449.5 jit_solution(236430586755640246)
XLA Ops:
  6.6 1.8 pad_maximum_fusion
  8.4 0.1 all-gather.4.cloned.1.call-update
  8.4 0.1 all-gather.6.cloned.1.call-start
  8.5 0.7 all-gather.6.cloned.1.call-update
  9.3 1.1 fusion.33
  10.3 0.6 broadcast_in_dim.12
  10.9 23.7 %all-to-all-start = ((f32[8,1,384]{2,1,0:T(1,128)}), f32[8,1,384]{2,1,0:T(1,128)S(1)}, u32[]{:S(2)}, u32[]{:S(2)}) async-start(f32[8,1,384]{2,1,0:T(1,128)} %broadcast_in_dim.12), calls=%async_computation | async-start | bytes 24576 | tf_op jit(solution)/shard_map/all_to_all | solution.py:15
  34.6 0.7 convert_element_type.81
  35.3 4.0 all-to-all-done
  39.4 0.1 fusion.35
  39.5 0.2 copy.33
  39.7 0.1 broadcast_in_dim.13
  39.8 23.8 %all_to_all.53 = bf16[8,384,256]{1,2,0:T(8,128)(2,1)S(1)} all-to-all(bf16[8,384,256]{1,2,0:T(8,128)(2,1)S(1)} %broadcast_in_dim.13), channel_id=1, replica_groups=mesh['grp'=2,'fs'=16,'tp'=8] {'tp'}, dimensions={0} | all-to-all | bytes 3145728 | tf_op jit(solution)/shard_map/all_to_all | solution.py:15
  63.6 55.7 %all-gather.4.cloned.1.call-done = bf16[2048,1408]{0,1:T(8,128)(2,1)} async-done(((bf16[128,1408]{0,1:T(8,128)(2,1)}), bf16[2048,1408]{0,1:T(8,128)(2,1)}) %all-gather.4.cloned.1.call-update) | async-done | bytes 5767184 | tf_op jit(solution)/shard_map/all_gather | solution.py:45
  119.4 4.5 %fusion.4 = f32[384,704]{0,1:T(8,128)} fusion(bf16[384,2048]{0,1:T(8,128)(2,1)S(1)} %bitcast.120, bf16[2048,1408]{0,1:T(8,128)(2,1)} %all-gather.4.cloned.1.call-done), kind=kOutput, calls=%fused_computation.10 | convolution fusion | flops 1107296256 | bytes 5537792 | tf_op jit(solution)/shard_map/dot_general | solution.py:90
  123.9 75.0 %all-gather.6.cloned.1.call-done = bf16[704,2048]{1,0:T(8,128)(2,1)} async-done(((bf16[704,128]{1,0:T(8,128)(2,1)}), bf16[704,2048]{1,0:T(8,128)(2,1)}) %all-gather.6.cloned.1.call-update) | async-done | bytes 2883600 | tf_op jit(solution)/shard_map/all_gather | solution.py:87
  198.9 6.0 %convolution_convert_fusion.1 = bf16[384,2048]{1,0:T(8,128)(2,1)S(1)} fusion(bf16[704,2048]{1,0:T(8,128)(2,1)} %all-gather.6.cloned.1.call-done, bf16[384,2048]{0,1:T(8,128)(2,1)S(1)} %bitcast.121, bf16[2048,1408]{0,1:T(8,128)(2,1)} %all-gather.4.cloned.1.call-done, f32[384,704]{0,1:T(8,128)} %fusion.4), kind=kOutput, calls=%fused_computation.4 | convolution fusion | flops 2217000960 | bytes 9994240 | tf_op jit(solution)/shard_map/dot_general | solution.py:93
  205.0 0.1 copy.53
  205.1 35.8 %all_to_all.54 = bf16[8,384,256]{2,1,0:T(8,128)(2,1)S(1)} all-to-all(bf16[8,384,256]{2,1,0:T(8,128)(2,1)S(1)} %bitcast.114), channel_id=1, replica_groups=mesh['grp'=2,'fs'=16,'tp'=8] {'tp'}, dimensions={0} | all-to-all | bytes 3145728 | tf_op jit(solution)/shard_map/all_to_all | solution.py:39
  240.9 0.2 convert_reduce_fusion.2
  241.1 0.2 fusion.37
  241.3 0.6 broadcast_in_dim.14
  241.9 4.3 all-to-all-start.3
  246.2 0.0 copy-done.6
  246.2 4.7 %all-to-all-done.3 = f32[8,1,384]{2,1,0:T(1,128)S(1)} async-done(((f32[8,1,384]{2,1,0:T(1,128)}), f32[8,1,384]{2,1,0:T(1,128)S(1)}, u32[]{:S(2)}, u32[]{:S(2)}) %all-to-all-start.3) | async-done | bytes 12320 | tf_op jit(solution)/shard_map/all_to_all | solution.py:15
  250.9 0.1 fusion.39
  251.0 0.2 copy.36
  251.2 1.3 broadcast_in_dim.15
  252.6 4.3 all-to-all-start.4
  256.9 0.1 all-gather.8.cloned.1.call-start
  257.0 0.0 copy-done.2
  257.0 0.0 copy-done.3
  257.0 0.6 pad_maximum_fusion.1
  257.6 0.1 all-gather.8.cloned.1.call-update
  257.7 0.1 copy.37
  257.8 19.7 %all-to-all-done.4 = bf16[8,384,256]{1,2,0:T(8,128)(2,1)S(1)} async-done(((bf16[8,384,256]{1,2,0:T(8,128)(2,1)}), bf16[8,384,256]{1,2,0:T(8,128)(2,1)S(1)}, u32[]{:S(2)}, u32[]{:S(2)}) %all-to-all-start.4) | async-done | bytes 1572896 | tf_op jit(solution)/shard_map/all_to_all | solution.py:15
  277.6 0.9 stack.2
  278.5 7.1 %all-to-all-start.5 = ((bf16[16,128,128]{1,2,0:T(8,128)(2,1)}), bf16[16,128,128]{1,2,0:T(8,128)(2,1)S(1)}, u32[]{:S(2)}, u32[]{:S(2)}) async-start(bf16[16,128,128]{1,2,0:T(8,128)(2,1)} %stack.2), calls=%async_computation.5 | async-start | bytes 1048576 | tf_op jit(solution)/shard_map/all_to_all | solution.py:119
  285.6 0.0 copy-done.7
  285.7 40.4 %all-gather.8.cloned.1.call-done = bf16[2048,256]{1,0:T(8,128)(2,1)} async-done(((bf16[128,256]{1,0:T(8,128)(2,1)}), bf16[2048,256]{1,0:T(8,128)(2,1)}) %all-gather.8.cloned.1.call-update) | async-done | bytes 1048592 | tf_op jit(solution)/shard_map/all_gather | solution.py:45
  326.1 1.7 fusion.31
  327.8 0.6 fusion.23
  328.5 0.7 fusion.107
  329.2 19.1 %all-reduce.1 = (f32[384]{0:T(512)S(1)}, f32[384]{0:T(512)S(1)}) all-reduce(f32[384]{0:T(512)S(1)} %bitcast.129, f32[384]{0:T(512)S(1)} %bitcast.128), channel_id=1, replica_groups=mesh['grp'=2,'fs'=16,'tp'=8] {'tp'}, use_global_device_ids=true, to_apply=%region_8.9 | all-reduce | flops 768 | bytes 6144 | tf_op jit(solution)/shard_map/psum | solution.py:109
  348.4 0.2 multiply_convert_fusion
  348.6 0.0 all-to-all-done.5
  348.6 0.6 convolution_convert_fusion.2
  349.2 0.1 copy.52
  349.3 23.7 %all_to_all.55 = bf16[8,384,256]{2,1,0:T(8,128)(2,1)S(1)} all-to-all(bf16[8,384,256]{2,1,0:T(8,128)(2,1)S(1)} %bitcast.115), channel_id=1, replica_groups=mesh['grp'=2,'fs'=16,'tp'=8] {'tp'}, dimensions={0} | all-to-all | bytes 3145728 | tf_op jit(solution)/shard_map/all_to_all | solution.py:39
  373.0 0.2 convert_reduce_fusion.1
  373.2 0.2 fusion.41
  373.4 0.6 broadcast_in_dim.32
  374.0 4.3 all-to-all-start.7
  378.3 4.7 %all-to-all-done.7 = f32[8,1,384]{2,1,0:T(1,128)S(1)} async-done(((f32[8,1,384]{2,1,0:T(1,128)}), f32[8,1,384]{2,1,0:T(1,128)S(1)}, u32[]{:S(2)}, u32[]{:S(2)}) %all-to-all-start.7) | async-done | bytes 12320 | tf_op jit(solution)/shard_map/all_to_all | solution.py:15
  383.0 0.1 fusion.43
  383.2 0.2 copy.40
  383.3 0.1 broadcast_in_dim.33
  383.5 23.8 %all_to_all.56 = bf16[8,384,256]{1,2,0:T(8,128)(2,1)S(1)} all-to-all(bf16[8,384,256]{1,2,0:T(8,128)(2,1)S(1)} %broadcast_in_dim.33), channel_id=1, replica_groups=mesh['grp'=2,'fs'=16,'tp'=8] {'tp'}, dimensions={0} | all-to-all | bytes 3145728 | tf_op jit(solution)/shard_map/all_to_all | solution.py:15
  407.3 4.5 %fusion.6 = f32[384,704]{0,1:T(8,128)} fusion(bf16[384,2048]{0,1:T(8,128)(2,1)S(1)} %bitcast.122, bf16[2048,1408]{0,1:T(8,128)(2,1)} %all-gather.4.cloned.1.call-done), kind=kOutput, calls=%fused_computation.12 | convolution fusion | flops 1107296256 | bytes 5537792 | tf_op jit(solution)/shard_map/dot_general | solution.py:90
  411.8 6.0 %convolution_convert_fusion = bf16[384,2048]{1,0:T(8,128)(2,1)S(1)} fusion(bf16[704,2048]{1,0:T(8,128)(2,1)} %all-gather.6.cloned.1.call-done, bf16[384,2048]{0,1:T(8,128)(2,1)S(1)} %bitcast.123, bf16[2048,1408]{0,1:T(8,128)(2,1)} %all-gather.4.cloned.1.call-done, f32[384,704]{0,1:T(8,128)} %fusion.6), kind=kOutput, calls=%fused_computation.3 | convolution fusion | flops 2217000960 | bytes 9994240 | tf_op jit(solution)/shard_map/dot_general | solution.py:93
  417.8 0.1 copy.51
  417.9 24.1 %all_to_all.57 = bf16[8,384,256]{2,1,0:T(8,128)(2,1)S(1)} all-to-all(bf16[8,384,256]{2,1,0:T(8,128)(2,1)S(1)} %bitcast.116), channel_id=1, replica_groups=mesh['grp'=2,'fs'=16,'tp'=8] {'tp'}, dimensions={0} | all-to-all | bytes 3145728 | tf_op jit(solution)/shard_map/all_to_all | solution.py:39
  442.0 0.2 convert_reduce_fusion
  442.3 0.7 fusion.44
  (31 shorter events, 0.2 us)
Async XLA Ops:
  6.5 32.8 %copy-start = (bf16[384,256]{1,0:T(8,128)(2,1)S(1)}, bf16[384,256]{1,0:T(8,128)(2,1)}, u32[]{:S(2)}) copy-start(bf16[384,256]{1,0:T(8,128)(2,1)} %param.13) | copy-start | bytes 589828
  6.5 112.8 %all-gather.4.cloned.1.call-start = ((), (), s32[]{:S(2)}) async-start(), calls=%async_computation.10 | async-start | bytes 6127616 | tf_op jit(solution)/shard_map/all_gather | solution.py:45
  8.4 190.5 %all-gather.6.cloned.1.call-start = ((), (), s32[]{:S(2)}) async-start(), calls=%async_computation.11 | async-start | bytes 3063808 | tf_op jit(solution)/shard_map/all_gather | solution.py:87
  10.9 28.4 %all-to-all-start = ((f32[8,1,384]{2,1,0:T(1,128)}), f32[8,1,384]{2,1,0:T(1,128)S(1)}, u32[]{:S(2)}, u32[]{:S(2)}) async-start(f32[8,1,384]{2,1,0:T(1,128)} %broadcast_in_dim.12), calls=%async_computation | async-start | bytes 24576 | tf_op jit(solution)/shard_map/all_to_all | solution.py:15
  240.9 5.3 %copy-start.6 = (bf16[256]{0:T(256)(128)(2,1)S(1)}, bf16[256]{0:T(256)(128)(2,1)}, u32[]{:S(2)}) copy-start(bf16[256]{0:T(256)(128)(2,1)} %param.15) | copy-start | bytes 1540
  241.9 9.0 %all-to-all-start.3 = ((f32[8,1,384]{2,1,0:T(1,128)}), f32[8,1,384]{2,1,0:T(1,128)S(1)}, u32[]{:S(2)}, u32[]{:S(2)}) async-start(f32[8,1,384]{2,1,0:T(1,128)} %broadcast_in_dim.14), calls=%async_computation.3 | async-start | bytes 24576 | tf_op jit(solution)/shard_map/all_to_all | solution.py:15
  252.6 4.4 copy-start.2
  252.6 4.4 copy-start.3
  252.6 5.1 %copy-start.1 = (bf16[128,128]{1,0:T(8,128)(2,1)S(1)}, bf16[128,128]{1,0:T(8,128)(2,1)}, u32[]{:S(2)}) copy-start(bf16[128,128]{1,0:T(8,128)(2,1)} %param.25) | copy-start | bytes 98308
  252.6 25.0 %all-to-all-start.4 = ((bf16[8,384,256]{1,2,0:T(8,128)(2,1)}), bf16[8,384,256]{1,2,0:T(8,128)(2,1)S(1)}, u32[]{:S(2)}, u32[]{:S(2)}) async-start(bf16[8,384,256]{1,2,0:T(8,128)(2,1)} %broadcast_in_dim.15), calls=%async_computation.4 | async-start | bytes 3145728 | tf_op jit(solution)/shard_map/all_to_all | solution.py:15
  256.9 28.7 %copy-start.4 = (bf16[31,128]{1,0:T(8,128)(2,1)S(1)}, bf16[31,128]{1,0:T(8,128)(2,1)}, u32[]{:S(2)}) copy-start(bf16[31,128]{1,0:T(8,128)(2,1)} %param.22) | copy-start | bytes 23812
  256.9 28.7 %copy-start.7 = (bf16[128]{0:T(256)(128)(2,1)S(1)}, bf16[128]{0:T(256)(128)(2,1)}, u32[]{:S(2)}) copy-start(bf16[128]{0:T(256)(128)(2,1)} %param.23) | copy-start | bytes 772
  256.9 28.7 %copy-start.8 = (bf16[128]{0:T(256)(128)(2,1)S(1)}, bf16[128]{0:T(256)(128)(2,1)}, u32[]{:S(2)}) copy-start(bf16[128]{0:T(256)(128)(2,1)} %param.24) | copy-start | bytes 772
  256.9 69.2 %all-gather.8.cloned.1.call-start = ((), (), s32[]{:S(2)}) async-start(), calls=%async_computation.12 | async-start | bytes 1114112 | tf_op jit(solution)/shard_map/all_gather | solution.py:45
  278.5 70.1 %all-to-all-start.5 = ((bf16[16,128,128]{1,2,0:T(8,128)(2,1)}), bf16[16,128,128]{1,2,0:T(8,128)(2,1)S(1)}, u32[]{:S(2)}, u32[]{:S(2)}) async-start(bf16[16,128,128]{1,2,0:T(8,128)(2,1)} %stack.2), calls=%async_computation.5 | async-start | bytes 1048576 | tf_op jit(solution)/shard_map/all_to_all | solution.py:119
  326.1 1.8 copy-start.5
  373.0 5.3 %copy-start.9 = (bf16[256]{0:T(256)(128)(2,1)S(1)}, bf16[256]{0:T(256)(128)(2,1)}, u32[]{:S(2)}) copy-start(bf16[256]{0:T(256)(128)(2,1)} %param.16) | copy-start | bytes 1540
  374.0 9.0 %all-to-all-start.7 = ((f32[8,1,384]{2,1,0:T(1,128)}), f32[8,1,384]{2,1,0:T(1,128)S(1)}, u32[]{:S(2)}, u32[]{:S(2)}) async-start(f32[8,1,384]{2,1,0:T(1,128)} %broadcast_in_dim.32), calls=%async_computation.7 | async-start | bytes 24576 | tf_op jit(solution)/shard_map/all_to_all | solution.py:15
Sparse Core Ops, SparseCore 0:
  9.1 110.2 all-gather.3
  121.1 77.7 all-gather.5
  259.5 66.4 all-gather.7
